TPU v7x, 512 devices: a whole 4x8x8 slice. The times are simulated.
512 devices in a mesh: ep: 32 (over z, x), tp: 16 (over y, core).
Axes of the slice: x: 4, y: 8, z: 8, core: 2. Of those that a mesh axis runs over, the one named last changes fastest.
Arguments:
- first_batch: bfloat16 [65536, 2048], P(('ep', 'tp')), may hold values from -6 to 6
- mixer_gain: float32 [2048], replicated, may hold values from 0.1 to 1.9
- mixer_in: bfloat16 [2048, 512], P(None, 'tp'), may hold values from -0.125 to 0.125
- group_maps: bfloat16 [8, 64, 64], replicated, may hold values from -0.75 to 0.75
- pool_scale: float32 [512], replicated, may hold values from 0.1 to 1.9
- mixer_out: bfloat16 [512, 2048], P('tp'), may hold values from -0.25 to 0.25
- second_batch: bfloat16 [4096, 2048], P('ep'), may hold values from -6 to 6
- expert_gain: float32 [2048], replicated, may hold values from 0.1 to 1.9
- expert_choice: int32 [4096, 2], P('ep'), may hold values from 0 to 31, all different within a row; in each aligned block of 128 rows (0 to 127, 128 to 255, ...) at most 16 rows name the same one
- route_scores: float32 [4096, 2], P('ep'), may hold values from -6 to 6
- expert_gate: bfloat16 [32, 2048, 3584], P('ep', None, 'tp'), may hold values from -0.125 to 0.125
- expert_up: bfloat16 [32, 2048, 3584], P('ep', None, 'tp'), may hold values from -0.125 to 0.125
- expert_down: bfloat16 [32, 3584, 2048], P('ep', 'tp'), may hold values from -0.09375 to 0.09375
Outputs:
- mixed_first: bfloat16 [65536, 2048], P(('ep', 'tp'))
- experts_second: bfloat16 [4096, 2048], P('ep')
Inputs may be any that keep to these rules, and one draw needn't show every extreme that they name: `expert_choice`: the two entries of a row differ. Within the rows of one device (aligned blocks of 128 rows) no expert is named more than 16 times, a bound that some block reaches there.
All inputs are finite; a program needn't handle non-finite values.
Results may differ from a plain program's by a relative error of at most 0.018.
Values may be sent and summed in bfloat16 or wider, within the bound.
No kernel may reach another device: no remote copies, remote signals or barrier semaphores. Data moves between devices by JAX's collectives and lax.ppermute only.
A program may use at most 64 MiB of HBM per device.

v0:
```python
import jax
import jax.numpy as jnp
from jax import lax
from jax.sharding import Mesh
from jax.sharding import PartitionSpec as P

GROUP = 64
SEQS = 1
EP_TP = ("ep_0", "ep_1", "tp")
EP = ("ep_0", "ep_1")
epsilon = 1e-06


def extended(block, sides, width):
    for axis, dim in sides:
        count = lax.axis_size(axis)
        forward = [(i, i + 1) for i in range(count - 1)]
        backward = [(target, source) for source, target in forward]
        low = lax.ppermute(
            lax.slice_in_dim(block, block.shape[dim] - width, None, axis=dim), axis, forward
        )
        high = lax.ppermute(lax.slice_in_dim(block, 0, width, axis=dim), axis, backward)
        block = jnp.concatenate([low, block, high], axis=dim)
    return block


def split_up(shard, dim, peers):
    lengths = shard.shape
    blocks = shard.reshape(*lengths[:dim], peers, lengths[dim] // peers, *lengths[dim + 1 :])
    return jnp.moveaxis(blocks, dim, 0)


def summed_on_arrival(shard, axis, dim):
    peers = lax.axis_size(axis)
    blocks = lax.all_to_all(split_up(shard, dim, peers), axis, 0, 0, tiled=True)
    return jnp.sum(blocks.astype(jnp.float32), axis=0)


def laid_out(blocks, dim):
    lengths = list(blocks.shape[1:])
    lengths[dim] *= blocks.shape[0]
    return jnp.moveaxis(blocks, 0, dim).reshape(lengths)


def moved_by_axis(blocks, axes, turns):
    inside = blocks.shape[1:]
    out = blocks.reshape(*(lax.axis_size(a) for a in axes), *inside)
    for k in turns:
        out = lax.all_to_all(out, axes[k], k, k, tiled=True)
    return out.reshape(-1, *inside)


def stepwise_exchange(shard, axes, turns, split_dim, concat_dim):
    blocks = split_up(shard, split_dim, lax.axis_size(axes))
    return laid_out(moved_by_axis(blocks, axes, turns), concat_dim)


def rms_scale(values, gain):
    floats = values.astype(jnp.float32)
    factor = lax.rsqrt(jnp.mean(floats * floats, axis=-1, keepdims=True) + epsilon)
    return (floats * factor * gain).astype(jnp.bfloat16)


def mixer_half(first_batch, mixer_gain, mixer_in, group_maps, pool_scale, mixer_out):
    count_rows = first_batch.shape[0]
    normed = rms_scale(first_batch, mixer_gain)
    pooled_in = jnp.dot(
        normed,
        lax.all_gather(mixer_in, "tp", axis=1, tiled=True),
        preferred_element_type=jnp.float32,
    ).astype(jnp.bfloat16)
    channels = pooled_in.shape[1]
    padded = extended(pooled_in, ((EP_TP, 0),), 8).astype(jnp.float32)
    devices = lax.axis_size(EP) * lax.axis_size("tp")
    seq_length = count_rows * devices // SEQS
    first_row = (lax.axis_index(EP) * lax.axis_size("tp") + lax.axis_index("tp")) * count_rows
    places = first_row + jnp.arange(count_rows, dtype=jnp.int32)
    own_seq = places // seq_length
    group_of = jnp.arange(channels, dtype=jnp.int32) // GROUP
    half_span = jnp.left_shift(jnp.ones_like(group_of), group_of % 4)
    window_sum = jnp.zeros((count_rows, channels), jnp.float32)
    window_count = jnp.zeros((count_rows, channels), jnp.float32)
    for offset in range(-8, 8):
        inside = (
            ((places + offset) // seq_length == own_seq)[:, None]
            & (offset >= -half_span)[None, :]
            & (offset < half_span)[None, :]
        )
        window_sum = window_sum + jnp.where(
            inside, padded[8 + offset : 8 + offset + count_rows], 0.0
        )
        window_count = window_count + inside.astype(jnp.float32)
    centred = (window_sum / window_count - padded[8 : 8 + count_rows]).astype(jnp.bfloat16)
    group_count = group_maps.shape[0]
    identity = jnp.eye(group_count, dtype=jnp.bfloat16)
    block_map = jnp.einsum("gcd,gh->gchd", group_maps, identity).reshape(channels, channels)
    grouped = (jnp.dot(centred, block_map, preferred_element_type=jnp.float32) * pool_scale).astype(
        jnp.bfloat16
    )
    mixed_out = jnp.dot(
        grouped,
        lax.all_gather(mixer_out, "tp", axis=0, tiled=True),
        preferred_element_type=jnp.float32,
    )
    return mixed_out.astype(jnp.bfloat16)


def expert_half(
    second_batch, expert_gain, expert_choice, route_scores, expert_gate, expert_up, expert_down
):
    row_count = second_batch.shape[0]
    model_width = second_batch.shape[1]
    experts = lax.axis_size(EP)
    tp_count = lax.axis_size("tp")
    capacity = 4 * row_count // experts
    share = capacity // tp_count
    normed = rms_scale(second_batch, expert_gain)
    chosen = expert_choice.reshape(-1)
    one_hot = (chosen[:, None] == jnp.arange(experts, dtype=jnp.int32)[None, :]).astype(jnp.int32)
    ranking = jnp.sum(jnp.cumsum(one_hot, axis=0) * one_hot, axis=1) - 1
    slot_place = ranking * experts + chosen
    source_row = jnp.arange(chosen.shape[0], dtype=jnp.int32) // expert_choice.shape[1]
    slot_table = jnp.zeros((capacity * experts,), jnp.int32).at[slot_place].set(source_row + 1)
    outgoing = jnp.where(
        (slot_table > 0)[:, None],
        normed[jnp.maximum(slot_table - 1, 0)],
        jnp.zeros((), jnp.bfloat16),
    )
    outgoing = outgoing.reshape(capacity, experts, model_width)
    arrived = lax.all_to_all(outgoing, EP, split_axis=1, concat_axis=1, tiled=True)
    incoming = arrived.reshape(capacity * experts, model_width)
    gate_weight = expert_gate[0]
    up_weight = expert_up[0]
    down_weight = expert_down[0]
    gate_part = jnp.dot(incoming, gate_weight, preferred_element_type=jnp.float32)
    up_part = jnp.dot(incoming, up_weight, preferred_element_type=jnp.float32)
    hidden = (jax.nn.silu(gate_part) * up_part).astype(jnp.bfloat16)
    summed = summed_on_arrival(
        jnp.dot(hidden, down_weight, preferred_element_type=jnp.float32).astype(jnp.bfloat16),
        "tp",
        0,
    )
    finished = summed.astype(jnp.bfloat16).reshape(share, experts, model_width)
    returned = stepwise_exchange(finished, EP, (0, 1), 1, 1)
    every_slot = lax.all_gather(returned, "tp", axis=0, tiled=True).reshape(
        capacity * experts, model_width
    )
    picked = every_slot[slot_place].reshape(row_count, -1, model_width)
    weight_first = jax.nn.sigmoid(route_scores[:, 0] - route_scores[:, 1])[:, None]
    blended = weight_first * picked[:, 0].astype(jnp.float32) + (1.0 - weight_first) * picked[
        :, 1
    ].astype(jnp.float32)
    return blended.astype(jnp.bfloat16)


def per_device(
    first_batch,
    mixer_gain,
    mixer_in,
    group_maps,
    pool_scale,
    mixer_out,
    second_batch,
    expert_gain,
    expert_choice,
    route_scores,
    expert_gate,
    expert_up,
    expert_down,
):
    mixed_first = mixer_half(first_batch, mixer_gain, mixer_in, group_maps, pool_scale, mixer_out)
    experts_second = expert_half(
        second_batch, expert_gain, expert_choice, route_scores, expert_gate, expert_up, expert_down
    )
    return (mixed_first, experts_second)


def solution(mesh):
    torus = Mesh(mesh.devices.reshape(8, 4, mesh.shape["tp"]), ("ep_0", "ep_1", "tp"))
    placed = (
        P(EP_TP, None),
        P(),
        P(None, "tp"),
        P(),
        P(),
        P("tp", None),
        P(EP, None),
        P(),
        P(EP, None),
        P(EP, None),
        P(EP, None, "tp"),
        P(EP, None, "tp"),
        P(EP, "tp", None),
    )
    return jax.shard_map(
        per_device,
        mesh=torus,
        in_specs=placed,
        out_specs=(P(EP_TP, None), P(EP, None)),
        check_vma=False,
    )
```

profile of v0, /device:TPU:1, one launch (start us, length us, event | category | flops | bytes accessed | tf_op | source)
XLA Modules:
  0.0 232.5 jit_solution(14111558558822395541)
XLA Ops:
  7.2 0.9 copy.31
  9.4 1.4 scatter_custom_fusion
  10.9 1.2 fusion.5
  12.3 1.2 fusion.7
  13.5 2.5 %gather_fusion = bf16[512,2048]{1,0:T(8,128)(2,1)S(1)} fusion(bf16[128,2048]{1,0:T(8,128)(2,1)S(1)} %fusion.7, s32[1024]{0:T(1024)S(1)} %pad_clamp_fusion.1), kind=kCustom, calls=%fused_computation | custom fusion | bytes 4196352 | tf_op jit(solution)/shard_map/gather | solution.py:126
  16.0 3.8 %copy_select_fusion = bf16[16,32,2048]{2,0,1:T(8,128)(2,1)} fusion(bf16[16,32,2048]{2,1,0:T(8,128)(2,1)S(1)} %bitcast.56, pred[16,32]{0,1:T(8,128)(4,1)S(1)} %copy.35), kind=kLoop, calls=%fused_computation.5 | loop fusion | flops 1048576 | bytes 4194816 | tf_op jit(solution)/shard_map/jit(_where)/select_n | solution.py:124
  19.8 13.7 %all-to-all-start = ((bf16[16,32,2048]{2,0,1:T(8,128)(2,1)}), bf16[16,32,2048]{2,0,1:T(8,128)(2,1)S(1)}, u32[]{:S(2)}, u32[]{:S(2)}) async-start(bf16[16,32,2048]{2,0,1:T(8,128)(2,1)} %copy_select_fusion), calls=%async_computation | async-start | bytes 4194304 | tf_op jit(solution)/shard_map/all_to_all | solution.py:130
  34.2 47.7 %all-to-all-done = bf16[16,32,2048]{2,0,1:T(8,128)(2,1)S(1)} async-done(((bf16[16,32,2048]{2,0,1:T(8,128)(2,1)}), bf16[16,32,2048]{2,0,1:T(8,128)(2,1)S(1)}, u32[]{:S(2)}, u32[]{:S(2)}) %all-to-all-start) | async-done | bytes 2097184 | tf_op jit(solution)/shard_map/all_to_all | solution.py:130
  82.0 1.2 copy.37
  83.1 1.3 copy-done.1
  84.5 0.8 fusion.13
  85.6 4.5 %convolution_convert_fusion = bf16[512,2048]{1,0:T(8,128)(2,1)} fusion(bf16[512,2048]{1,0:T(8,128)(2,1)} %bitcast.59, bf16[1,224,2048]{2,1,0:T(8,128)(2,1)S(1)} %copy-done, bf16[1,2048,224]{1,2,0:T(8,128)(2,1)S(1)} %copy-done.6, f32[512,224]{0,1:T(8,128)S(1)} %fusion.13), kind=kOutput, calls=%fused_computation.3 | convolution fusion | flops 941260800 | bytes 6488064 | tf_op jit(solution)/shard_map/dot_general | solution.py:139
  90.1 9.8 %all-to-all-start.1 = ((bf16[16,32,2048]{2,1,0:T(8,128)(2,1)}), bf16[16,32,2048]{2,1,0:T(8,128)(2,1)S(1)}, u32[]{:S(2)}, u32[]{:S(2)}) async-start(bf16[16,32,2048]{2,1,0:T(8,128)(2,1)} %bitcast.57), calls=%async_computation.1 | async-start | bytes 4194304 | tf_op jit(solution)/shard_map/all_to_all | solution.py:35
  99.9 0.7 all-gather.6.cloned.1.call-update
  100.8 56.7 %all-to-all-done.1 = bf16[16,32,2048]{2,1,0:T(8,128)(2,1)S(1)} async-done(((bf16[16,32,2048]{2,1,0:T(8,128)(2,1)}), bf16[16,32,2048]{2,1,0:T(8,128)(2,1)S(1)}, u32[]{:S(2)}, u32[]{:S(2)}) %all-to-all-start.1) | async-done | bytes 2097184 | tf_op jit(solution)/shard_map/all_to_all | solution.py:35
  157.9 0.7 reshape_transpose_reshape_reshape.3
  158.6 3.7 %all-to-all-start.2 = ((bf16[8,4,1,1,2048]{4,1,3,2,0:T(4,128)(2,1)}), bf16[8,4,1,1,2048]{4,1,3,2,0:T(4,128)(2,1)S(1)}, u32[]{:S(2)}, u32[]{:S(2)}) async-start(bf16[8,4,1,1,2048]{4,1,3,2,0:T(4,128)(2,1)} %reshape_transpose_reshape_reshape.3), calls=%async_computation.2 | async-start | bytes 262144 | tf_op jit(solution)/shard_map/all_to_all | solution.py:49
  162.4 7.9 %all-to-all-done.2 = bf16[8,4,1,1,2048]{4,1,3,2,0:T(4,128)(2,1)S(1)} async-done(((bf16[8,4,1,1,2048]{4,1,3,2,0:T(4,128)(2,1)}), bf16[8,4,1,1,2048]{4,1,3,2,0:T(4,128)(2,1)S(1)}, u32[]{:S(2)}, u32[]{:S(2)}) %all-to-all-start.2) | async-done | bytes 131104 | tf_op jit(solution)/shard_map/all_to_all | solution.py:49
  170.3 0.7 copy.38
  171.0 3.5 %all-to-all-start.3 = ((bf16[8,4,1,1,2048]{4,0,3,2,1:T(8,128)(2,1)}), bf16[8,4,1,1,2048]{4,0,3,2,1:T(8,128)(2,1)S(1)}, u32[]{:S(2)}, u32[]{:S(2)}) async-start(bf16[8,4,1,1,2048]{4,0,3,2,1:T(8,128)(2,1)} %copy.38), calls=%async_computation.3 | async-start | bytes 262144 | tf_op jit(solution)/shard_map/all_to_all | solution.py:49
  174.6 4.7 %all-to-all-done.3 = bf16[8,4,1,1,2048]{4,0,3,2,1:T(8,128)(2,1)S(1)} async-done(((bf16[8,4,1,1,2048]{4,0,3,2,1:T(8,128)(2,1)}), bf16[8,4,1,1,2048]{4,0,3,2,1:T(8,128)(2,1)S(1)}, u32[]{:S(2)}, u32[]{:S(2)}) %all-to-all-start.3) | async-done | bytes 131104 | tf_op jit(solution)/shard_map/all_to_all | solution.py:49
  179.4 0.7 reshape_transpose_reshape.3
  180.8 2.4 %convolution_convert_fusion.2 = bf16[128,512]{1,0:T(8,128)(2,1)S(1)} fusion(bf16[2048,512]{0,1:T(8,128)(2,1)} %all-gather.4.cloned.1.call-done, bf16[128,2048]{1,0:T(8,128)(2,1)S(1)} %copy-done.2, f32[2048]{0:T(1024)S(1)} %copy-done.7, f32[128]{0:T(128)S(1)} %add_rsqrt_fusion.1), kind=kOutput, calls=%fused_computation.14 | convolution fusion | flops 269549568 | bytes 2761216 | tf_op jit(solution)/shard_map/dot_general | solution.py:67
  183.3 6.1 %collective-permute-start = (bf16[8,512]{1,0:T(8,128)(2,1)S(1)}, bf16[8,512]{1,0:T(8,128)(2,1)S(1)}, u32[]{:S(2)}, u32[]{:S(2)}) collective-permute-start(bf16[8,512]{1,0:T(8,128)(2,1)S(1)} %get-tuple-element.6), channel_id=1, source_target_pairs={{0,1},{1,2},{2,3},{3,4},{4,5},{5,6},{6,7},{7,8},{8,9},{9,10},{10,1... | collective-permute-start | bytes 24584 | tf_op jit(solution)/shard_map/ppermute | solution.py:19
  189.4 1.9 collective-permute-start.1
  192.0 2.5 %collective-permute-done.1 = bf16[8,512]{1,0:T(8,128)(2,1)S(1)} collective-permute-done((bf16[8,512]{1,0:T(8,128)(2,1)S(1)}, bf16[8,512]{1,0:T(8,128)(2,1)S(1)}, u32[]{:S(2)}, u32[]{:S(2)}) %collective-permute-start.1) | collective-permute-done | bytes 8224 | tf_op jit(solution)/shard_map/ppermute | solution.py:22
  194.5 4.2 %convolution_convert_fusion.1 = bf16[128,2048]{1,0:T(8,128)(2,1)} fusion(bf16[512,2048]{1,0:T(8,128)(2,1)} %all-gather.6.cloned.1.call-done, bf16[512,512]{1,0:T(8,128)(2,1)S(1)} %reshape.526, f32[144,512]{1,0:T(8,128)S(1)} %maximum_convert_fusion, f32[512]{0:T(512)S(1)} %copy-done.8, f32[512]{0:T(512)S(1)} %get-tuple-element.53, ...), kind=kOutput, calls=%fused_computation.4 | convolution fusion | flops 342097920 | bytes 7367680 | tf_op jit(solution)/shard_map/dot_general | solution.py:100
  198.8 18.9 %all-gather.8.cloned.1.call-done = bf16[16,32,2048]{2,1,0:T(8,128)(2,1)} async-done(((bf16[1,32,2048]{2,1,0:T(8,128)(2,1)}), bf16[16,32,2048]{2,1,0:T(8,128)(2,1)}) %all-gather.8.cloned.1.call-update) | async-done | bytes 2097168 | tf_op jit(solution)/shard_map/all_gather | solution.py:145
  217.7 4.2 %gather_fusion.1 = bf16[256,2048]{1,0:T(8,128)(2,1)S(1)} fusion(bf16[512,2048]{1,0:T(8,128)(2,1)} %bitcast.55, s32[1024]{0:T(1024)S(1)} %pad_clamp_fusion), kind=kCustom, calls=%fused_computation.1 | custom fusion | bytes 2098176 | tf_op jit(solution)/shard_map/gather | solution.py:148
  221.9 0.7 reshape.532
  222.7 1.5 fusion.173
  224.2 1.8 fusion.9
  (78 shorter events, 4.6 us)
Async XLA Ops:
  7.2 78.1 %copy-start = (bf16[1,224,2048]{2,1,0:T(8,128)(2,1)S(1)}, bf16[1,224,2048]{2,1,0:T(8,128)(2,1)}, u32[]{:S(2)}) copy-start(bf16[1,224,2048]{2,1,0:T(8,128)(2,1)} %param.25) | copy-start | bytes 2752516
  19.8 62.2 %all-to-all-start = ((bf16[16,32,2048]{2,0,1:T(8,128)(2,1)}), bf16[16,32,2048]{2,0,1:T(8,128)(2,1)S(1)}, u32[]{:S(2)}, u32[]{:S(2)}) async-start(bf16[16,32,2048]{2,0,1:T(8,128)(2,1)} %copy_select_fusion), calls=%async_computation | async-start | bytes 4194304 | tf_op jit(solution)/shard_map/all_to_all | solution.py:130
  33.5 147.3 %all-gather.4.cloned.1.call-start = ((), (), s32[]{:S(2)}) async-start(), calls=%async_computation.4 | async-start | bytes 2228224 | tf_op jit(solution)/shard_map/all_gather | solution.py:69
  82.0 2.5 %copy-start.5 = (bf16[1,2048,224]{1,2,0:T(8,128)(2,1)S(1)}, bf16[1,2048,224]{1,2,0:T(8,128)(2,1)}, u32[]{:S(2)}) copy-start(bf16[1,2048,224]{1,2,0:T(8,128)(2,1)} %param.23) | copy-start | bytes 2752516
  83.1 1.3 copy-start.1
  84.5 1.2 copy-start.6
  90.1 67.3 %all-to-all-start.1 = ((bf16[16,32,2048]{2,1,0:T(8,128)(2,1)}), bf16[16,32,2048]{2,1,0:T(8,128)(2,1)S(1)}, u32[]{:S(2)}, u32[]{:S(2)}) async-start(bf16[16,32,2048]{2,1,0:T(8,128)(2,1)} %bitcast.57), calls=%async_computation.1 | async-start | bytes 4194304 | tf_op jit(solution)/shard_map/all_to_all | solution.py:35
  99.9 94.6 %all-gather.6.cloned.1.call-start = ((), (), s32[]{:S(2)}) async-start(), calls=%async_computation.5 | async-start | bytes 2228224 | tf_op jit(solution)/shard_map/all_gather | solution.py:102
  100.7 79.8 %copy-start.4 = (f32[128,2]{0,1:T(2,128)S(1)}, f32[128,2]{0,1:T(2,128)}, u32[]{:S(2)}) copy-start(f32[128,2]{0,1:T(2,128)} %param.22) | copy-start | bytes 3076
  100.8 79.8 %copy-start.3 = (bf16[8,64,64]{2,1,0:T(8,128)(2,1)S(1)}, bf16[8,64,64]{2,1,0:T(8,128)(2,1)}, u32[]{:S(2)}) copy-start(bf16[8,64,64]{2,1,0:T(8,128)(2,1)} %param.16) | copy-start | bytes 196612
  157.9 22.5 %copy-start.2 = (bf16[128,2048]{1,0:T(8,128)(2,1)S(1)}, bf16[128,2048]{1,0:T(8,128)(2,1)}, u32[]{:S(2)}) copy-start(bf16[128,2048]{1,0:T(8,128)(2,1)} %param.13) | copy-start | bytes 1572868
  157.9 22.9 %copy-start.7 = (f32[2048]{0:T(1024)S(1)}, f32[2048]{0:T(1024)}, u32[]{:S(2)}) copy-start(f32[2048]{0:T(1024)} %param.14) | copy-start | bytes 24580
  158.6 11.6 %all-to-all-start.2 = ((bf16[8,4,1,1,2048]{4,1,3,2,0:T(4,128)(2,1)}), bf16[8,4,1,1,2048]{4,1,3,2,0:T(4,128)(2,1)S(1)}, u32[]{:S(2)}, u32[]{:S(2)}) async-start(bf16[8,4,1,1,2048]{4,1,3,2,0:T(4,128)(2,1)} %reshape_transpose_reshape_reshape.3), calls=%async_computation.2 | async-start | bytes 262144 | tf_op jit(solution)/shard_map/all_to_all | solution.py:49
  171.0 8.3 %all-to-all-start.3 = ((bf16[8,4,1,1,2048]{4,0,3,2,1:T(8,128)(2,1)}), bf16[8,4,1,1,2048]{4,0,3,2,1:T(8,128)(2,1)S(1)}, u32[]{:S(2)}, u32[]{:S(2)}) async-start(bf16[8,4,1,1,2048]{4,0,3,2,1:T(8,128)(2,1)} %copy.38), calls=%async_computation.3 | async-start | bytes 262144 | tf_op jit(solution)/shard_map/all_to_all | solution.py:49
  174.5 43.2 %all-gather.8.cloned.1.call-start = ((), (), s32[]{:S(2)}) async-start(), calls=%async_computation.6 | async-start | bytes 2228224 | tf_op jit(solution)/shard_map/all_gather | solution.py:145
  180.8 13.8 %copy-start.8 = (f32[512]{0:T(512)S(1)}, f32[512]{0:T(512)}, u32[]{:S(2)}) copy-start(f32[512]{0:T(512)} %param.17) | copy-start | bytes 6148
  183.3 8.7 %collective-permute-start = (bf16[8,512]{1,0:T(8,128)(2,1)S(1)}, bf16[8,512]{1,0:T(8,128)(2,1)S(1)}, u32[]{:S(2)}, u32[]{:S(2)}) collective-permute-start(bf16[8,512]{1,0:T(8,128)(2,1)S(1)} %get-tuple-element.6), channel_id=1, source_target_pairs={{0,1},{1,2},{2,3},{3,4},{4,5},{5,6},{6,7},{7,8},{8,9},{9,10},{10,1... | collective-permute-start | bytes 24584 | tf_op jit(solution)/shard_map/ppermute | solution.py:19
  189.4 5.1 %collective-permute-start.1 = (bf16[8,512]{1,0:T(8,128)(2,1)S(1)}, bf16[8,512]{1,0:T(8,128)(2,1)S(1)}, u32[]{:S(2)}, u32[]{:S(2)}) collective-permute-start(bf16[8,512]{1,0:T(8,128)(2,1)S(1)} %get-tuple-element.7), channel_id=1, source_target_pairs={{1,0},{2,1},{3,2},{4,3},{5,4},{6,5},{7,6},{8,7},{9,8},{10,9},{11,1... | collective-permute-start | bytes 24584 | tf_op jit(solution)/shard_map/ppermute | solution.py:22
Sparse Core Ops, SparseCore 0:
  36.4 43.6 all-gather.3
  102.8 57.5 all-gather.5
  180.2 37.4 all-gather.7
where the time goes:
time: 233 us; the launch traced here: 232 us
  waiting for transfers between devices  140 us (60%)
  starting transfers between devices  38.8 us (17%)
  local copies, waits for them, and re-layouts  17.7 us (8%)
  between operations  14.2 us (6%)
  matrix products  12 us (5%)
  other arithmetic  9.87 us (4%)
    all_to_all x1, waiting for transfers between devices, summed_on_arrival(): blocks = lax.all_to_all(split_up(shard, dim, peers), axis, 0, 0, tiled=True)  56.7 us
    all_to_all x1, waiting for transfers between devices, expert_half(): lax.all_to_all(outgoing, EP, split_axis=1, concat_axis=1, tiled=True)  47.7 us
    all_gather x1, waiting for transfers between devices, expert_half(): lax.all_gather(returned, 'tp', axis=0, tiled=True)  18.9 us
    all_to_all x1, starting transfers between devices, expert_half(): lax.all_to_all(outgoing, EP, split_axis=1, concat_axis=1, tiled=True)  13.7 us
    all_to_all x2, waiting for transfers between devices, moved_by_axis(): out = lax.all_to_all(out, axes[k], k, k, tiled=True)  12.6 us
    all_to_all x1, starting transfers between devices, summed_on_arrival(): blocks = lax.all_to_all(split_up(shard, dim, peers), axis, 0, 0, tiled=True)  9.75 us
    all_to_all x2, starting transfers between devices, moved_by_axis(): out = lax.all_to_all(out, axes[k], k, k, tiled=True)  7.19 us
    ppermute x1, starting transfers between devices, extended(): lax.ppermute(lax.slice_in_dim(block, block.shape[dim] - width, None, axis...  6.09 us
  transfers between devices with their start and end apart: 9, of which 6 were waited for; matrix products, arithmetic and copies ran while one was open for 7% of the time, Pallas kernels for 0%

commit v1 on v0

--- a/solution.py
+++ b/solution.py
@@ -9,6 +9,13 @@
 EP_TP = ("ep_0", "ep_1", "tp")
 EP = ("ep_0", "ep_1")
 epsilon = 1e-06
+
+
+def gather_over(x, name, dim):
+    n_dev = lax.axis_size(name)
+    blocks = jnp.stack([x for _ in range(n_dev)])
+    blocks = lax.all_to_all(blocks, name, split_axis=0, concat_axis=0)
+    return jnp.concatenate(blocks, axis=dim)
 
 
 def extended(block, sides, width):
@@ -142,9 +149,7 @@
     )
     finished = summed.astype(jnp.bfloat16).reshape(share, experts, model_width)
     returned = stepwise_exchange(finished, EP, (0, 1), 1, 1)
-    every_slot = lax.all_gather(returned, "tp", axis=0, tiled=True).reshape(
-        capacity * experts, model_width
-    )
+    every_slot = gather_over(returned, "tp", 0).reshape(capacity * experts, model_width)
     picked = every_slot[slot_place].reshape(row_count, -1, model_width)
     weight_first = jax.nn.sigmoid(route_scores[:, 0] - route_scores[:, 1])[:, None]
     blended = weight_first * picked[:, 0].astype(jnp.float32) + (1.0 - weight_first) * picked[

time: 233 us -> 261 us (1.12)
  other arithmetic: 9.87 us -> 28.1 us
  starting transfers between devices: 38.8 us -> 44.8 us
    ppermute x1, waiting for transfers between devices: 0.01 us -> 22.3 us  [extended(): lax.ppermute(lax.slice_in_dim(block, block.shape[dim] - width, None, axis...]
    all_gather x1 -> x0, waiting for transfers between devices: 18.9 us -> none  [expert_half(): lax.all_gather(returned, 'tp', axis=0, tiled=True)]
    all_to_all x0 -> x1, starting transfers between devices: none -> 8.65 us  [gather_over(): blocks = lax.all_to_all(blocks, name, split_axis=0, concat_axis=0)]
    le x14, other arithmetic: 0.12 us -> 7.9 us  [mixer_half(): offset >= -half_span]
    eq x8, other arithmetic: 0.13 us -> 4.74 us  [mixer_half(): (places + offset) // seq_length == own_seq]
  transfers between devices with their start and end apart: 9 -> 9, of which waited for: 6 -> 6; matrix products, arithmetic and copies ran while one was open for 7% -> 16% of each run, Pallas kernels for 0% -> 0%
where the time goes in v1:
time: 261 us; the launch traced here: 260 us
  waiting for transfers between devices  139 us (53%)
  starting transfers between devices  44.8 us (17%)
  other arithmetic  28.1 us (11%)
  local copies, waits for them, and re-layouts  19.9 us (8%)
  matrix products  14.3 us (5%)
  between operations  14.3 us (5%)
    all_to_all x1, waiting for transfers between devices, summed_on_arrival(): blocks = lax.all_to_all(split_up(shard, dim, peers), axis, 0, 0, tiled=True)  54.4 us
    all_to_all x1, waiting for transfers between devices, expert_half(): lax.all_to_all(outgoing, EP, split_axis=1, concat_axis=1, tiled=True)  47.7 us
    ppermute x1, waiting for transfers between devices, extended(): lax.ppermute(lax.slice_in_dim(block, block.shape[dim] - width, None, axis...  22.3 us
    all_to_all x1, starting transfers between devices, expert_half(): lax.all_to_all(outgoing, EP, split_axis=1, concat_axis=1, tiled=True)  13.7 us
    all_to_all x2, waiting for transfers between devices, moved_by_axis(): out = lax.all_to_all(out, axes[k], k, k, tiled=True)  10.4 us
    all_to_all x1, starting transfers between devices, summed_on_arrival(): blocks = lax.all_to_all(split_up(shard, dim, peers), axis, 0, 0, tiled=True)  9.75 us
    all_to_all x1, starting transfers between devices, gather_over(): blocks = lax.all_to_all(blocks, name, split_axis=0, concat_axis=0)  8.65 us
    le x14, other arithmetic, mixer_half(): offset >= -half_span  7.9 us
  transfers between devices with their start and end apart: 9, of which 6 were waited for; matrix products, arithmetic and copies ran while one was open for 16% of the time, Pallas kernels for 0%

profile of v1, /device:TPU:1, one launch (start us, length us, event | category | flops | bytes accessed | tf_op | source)
XLA Modules:
  0.0 260.3 jit_solution(1649798705841614774)
XLA Ops:
  7.2 0.9 copy.31
  9.4 1.4 scatter_custom_fusion
  10.9 1.2 fusion.5
  12.3 1.2 fusion.7
  13.5 2.5 gather_fusion
  16.0 3.8 %copy_select_fusion = bf16[16,32,2048]{2,0,1:T(8,128)(2,1)} fusion(bf16[16,32,2048]{2,1,0:T(8,128)(2,1)S(1)} %bitcast.56, pred[16,32]{0,1:T(8,128)(4,1)S(1)} %copy.35), kind=kLoop, calls=%fused_computation.5 | loop fusion | flops 1048576 | bytes 4194816 | tf_op jit(solution)/shard_map/jit(_where)/select_n | solution.py:131
  19.8 13.7 %all-to-all-start = ((bf16[16,32,2048]{2,0,1:T(8,128)(2,1)}), bf16[16,32,2048]{2,0,1:T(8,128)(2,1)S(1)}, u32[]{:S(2)}, u32[]{:S(2)}) async-start(bf16[16,32,2048]{2,0,1:T(8,128)(2,1)} %copy_select_fusion), calls=%async_computation | async-start | bytes 4194304 | tf_op jit(solution)/shard_map/all_to_all | solution.py:137
  34.3 47.7 %all-to-all-done = bf16[16,32,2048]{2,0,1:T(8,128)(2,1)S(1)} async-done(((bf16[16,32,2048]{2,0,1:T(8,128)(2,1)}), bf16[16,32,2048]{2,0,1:T(8,128)(2,1)S(1)}, u32[]{:S(2)}, u32[]{:S(2)}) %all-to-all-start) | async-done | bytes 2097184 | tf_op jit(solution)/shard_map/all_to_all | solution.py:137
  82.0 1.2 copy.37
  83.2 1.4 copy-done.1
  85.7 4.5 %convolution_convert_fusion = bf16[512,2048]{1,0:T(8,128)(2,1)} fusion(bf16[512,2048]{1,0:T(8,128)(2,1)} %bitcast.59, bf16[1,224,2048]{2,1,0:T(8,128)(2,1)S(1)} %copy-done, bf16[1,2048,224]{1,2,0:T(8,128)(2,1)S(1)} %copy-done.8, f32[512,224]{0,1:T(8,128)S(1)} %fusion.13), kind=kOutput, calls=%fused_computation.3 | convolution fusion | flops 941260800 | bytes 6488064 | tf_op jit(solution)/shard_map/dot_general | solution.py:146
  90.2 9.8 %all-to-all-start.1 = ((bf16[16,32,2048]{2,1,0:T(8,128)(2,1)}), bf16[16,32,2048]{2,1,0:T(8,128)(2,1)S(1)}, u32[]{:S(2)}, u32[]{:S(2)}) async-start(bf16[16,32,2048]{2,1,0:T(8,128)(2,1)} %bitcast.57), calls=%async_computation.1 | async-start | bytes 4194304 | tf_op jit(solution)/shard_map/all_to_all | solution.py:42
  103.1 54.4 %all-to-all-done.1 = bf16[16,32,2048]{2,1,0:T(8,128)(2,1)S(1)} async-done(((bf16[16,32,2048]{2,1,0:T(8,128)(2,1)}), bf16[16,32,2048]{2,1,0:T(8,128)(2,1)S(1)}, u32[]{:S(2)}, u32[]{:S(2)}) %all-to-all-start.1) | async-done | bytes 2097184 | tf_op jit(solution)/shard_map/all_to_all | solution.py:42
  158.7 3.7 %all-to-all-start.2 = ((bf16[8,4,1,1,2048]{4,1,3,2,0:T(4,128)(2,1)}), bf16[8,4,1,1,2048]{4,1,3,2,0:T(4,128)(2,1)S(1)}, u32[]{:S(2)}, u32[]{:S(2)}) async-start(bf16[8,4,1,1,2048]{4,1,3,2,0:T(4,128)(2,1)} %reshape_transpose_reshape_reshape.3), calls=%async_computation.2 | async-start | bytes 262144 | tf_op jit(solution)/shard_map/all_to_all | solution.py:56
  164.2 6.1 %all-to-all-done.2 = bf16[8,4,1,1,2048]{4,1,3,2,0:T(4,128)(2,1)S(1)} async-done(((bf16[8,4,1,1,2048]{4,1,3,2,0:T(4,128)(2,1)}), bf16[8,4,1,1,2048]{4,1,3,2,0:T(4,128)(2,1)S(1)}, u32[]{:S(2)}, u32[]{:S(2)}) %all-to-all-start.2) | async-done | bytes 131104 | tf_op jit(solution)/shard_map/all_to_all | solution.py:56
  171.0 3.5 %all-to-all-start.3 = ((bf16[8,4,1,1,2048]{4,0,3,2,1:T(8,128)(2,1)}), bf16[8,4,1,1,2048]{4,0,3,2,1:T(8,128)(2,1)S(1)}, u32[]{:S(2)}, u32[]{:S(2)}) async-start(bf16[8,4,1,1,2048]{4,0,3,2,1:T(8,128)(2,1)} %copy.38), calls=%async_computation.3 | async-start | bytes 262144 | tf_op jit(solution)/shard_map/all_to_all | solution.py:56
  175.1 4.2 %all-to-all-done.3 = bf16[8,4,1,1,2048]{4,0,3,2,1:T(8,128)(2,1)S(1)} async-done(((bf16[8,4,1,1,2048]{4,0,3,2,1:T(8,128)(2,1)}), bf16[8,4,1,1,2048]{4,0,3,2,1:T(8,128)(2,1)S(1)}, u32[]{:S(2)}, u32[]{:S(2)}) %all-to-all-start.3) | async-done | bytes 131104 | tf_op jit(solution)/shard_map/all_to_all | solution.py:56
  179.5 1.6 stack.3
  181.1 8.6 %all-to-all-start.4 = ((bf16[16,1,32,2048]{3,2,1,0:T(8,128)(2,1)}), bf16[16,1,32,2048]{3,2,1,0:T(8,128)(2,1)S(1)}, u32[]{:S(2)}, u32[]{:S(2)}) async-start(bf16[16,1,32,2048]{3,2,1,0:T(8,128)(2,1)} %stack.3), calls=%async_computation.4 | async-start | bytes 4194304 | tf_op jit(solution)/shard_map/all_to_all | solution.py:17
  199.6 2.0 multiply_bitcast_fusion
  201.6 2.4 convolution_convert_fusion.2
  204.7 3.5 %collective-permute-start = (bf16[8,512]{1,0:T(8,128)(2,1)}, bf16[8,512]{1,0:T(8,128)(2,1)S(1)}, u32[]{:S(2)}, u32[]{:S(2)}) collective-permute-start(bf16[8,512]{1,0:T(8,128)(2,1)} %get-tuple-element.6), channel_id=1, source_target_pairs={{0,1},{1,2},{2,3},{3,4},{4,5},{5,6},{6,7},{7,8},{8,9},{9,10},{10,1... | collective-permute-start | bytes 24584 | tf_op jit(solution)/shard_map/ppermute | solution.py:26
  208.3 1.9 collective-permute-start.1
  210.7 1.9 reshape.527
  212.6 22.3 %collective-permute-done = bf16[8,512]{1,0:T(8,128)(2,1)S(1)} collective-permute-done((bf16[8,512]{1,0:T(8,128)(2,1)}, bf16[8,512]{1,0:T(8,128)(2,1)S(1)}, u32[]{:S(2)}, u32[]{:S(2)}) %collective-permute-start) | collective-permute-done | bytes 8224 | tf_op jit(solution)/shard_map/ppermute | solution.py:26
  234.9 2.8 %collective-permute-done.1 = bf16[8,512]{1,0:T(8,128)(2,1)S(1)} collective-permute-done((bf16[8,512]{1,0:T(8,128)(2,1)}, bf16[8,512]{1,0:T(8,128)(2,1)S(1)}, u32[]{:S(2)}, u32[]{:S(2)}) %collective-permute-start.1) | collective-permute-done | bytes 8224 | tf_op jit(solution)/shard_map/ppermute | solution.py:29
  237.7 1.6 maximum_convert_fusion
  239.3 6.6 %convolution_convert_fusion.1 = bf16[128,2048]{1,0:T(8,128)(2,1)} fusion(bf16[512,2048]{1,0:T(8,128)(2,1)} %all-gather.5.cloned.1.call-done, bf16[512,512]{1,0:T(8,128)(2,1)S(1)} %reshape.527, f32[144,512]{1,0:T(8,128)} %maximum_convert_fusion, f32[512]{0:T(512)} %param.17, f32[512]{0:T(512)} %get-tuple-element.53, pred[512]{0:T(512)(128)(4,1)} %get-tuple-element.23, ...), kind=kOutput, calls=%fused_computation.4 | convolution fusion | flops 342097920 | bytes 7367680 | tf_op jit(solution)/shard_map/dot_general | solution.py:107
  245.9 2.5 gather_fusion.1
  248.4 1.7 reshape.532
  250.2 1.5 fusion.173
  251.7 1.8 fusion.9
  (78 shorter events, 22.0 us)
Async XLA Ops:
  7.2 78.2 %copy-start = (bf16[1,224,2048]{2,1,0:T(8,128)(2,1)S(1)}, bf16[1,224,2048]{2,1,0:T(8,128)(2,1)}, u32[]{:S(2)}) copy-start(bf16[1,224,2048]{2,1,0:T(8,128)(2,1)} %param.25) | copy-start | bytes 2752516
  19.8 62.2 %all-to-all-start = ((bf16[16,32,2048]{2,0,1:T(8,128)(2,1)}), bf16[16,32,2048]{2,0,1:T(8,128)(2,1)S(1)}, u32[]{:S(2)}, u32[]{:S(2)}) async-start(bf16[16,32,2048]{2,0,1:T(8,128)(2,1)} %copy_select_fusion), calls=%async_computation | async-start | bytes 4194304 | tf_op jit(solution)/shard_map/all_to_all | solution.py:137
  33.5 168.1 %all-gather.3.cloned.1.call-start = ((), (), s32[]{:S(2)}) async-start(), calls=%async_computation.5 | async-start | bytes 2228224 | tf_op jit(solution)/shard_map/all_gather | solution.py:76
  82.0 2.5 copy-start.7
  83.2 1.4 copy-start.1
  84.5 1.2 copy-start.8
  90.2 67.3 %all-to-all-start.1 = ((bf16[16,32,2048]{2,1,0:T(8,128)(2,1)}), bf16[16,32,2048]{2,1,0:T(8,128)(2,1)S(1)}, u32[]{:S(2)}, u32[]{:S(2)}) async-start(bf16[16,32,2048]{2,1,0:T(8,128)(2,1)} %bitcast.57), calls=%async_computation.1 | async-start | bytes 4194304 | tf_op jit(solution)/shard_map/all_to_all | solution.py:42
  100.0 139.3 %all-gather.5.cloned.1.call-start = ((), (), s32[]{:S(2)}) async-start(), calls=%async_computation.6 | async-start | bytes 2228224 | tf_op jit(solution)/shard_map/all_gather | solution.py:109
  158.7 11.6 %all-to-all-start.2 = ((bf16[8,4,1,1,2048]{4,1,3,2,0:T(4,128)(2,1)}), bf16[8,4,1,1,2048]{4,1,3,2,0:T(4,128)(2,1)S(1)}, u32[]{:S(2)}, u32[]{:S(2)}) async-start(bf16[8,4,1,1,2048]{4,1,3,2,0:T(4,128)(2,1)} %reshape_transpose_reshape_reshape.3), calls=%async_computation.2 | async-start | bytes 262144 | tf_op jit(solution)/shard_map/all_to_all | solution.py:56
  171.0 8.3 %all-to-all-start.3 = ((bf16[8,4,1,1,2048]{4,0,3,2,1:T(8,128)(2,1)}), bf16[8,4,1,1,2048]{4,0,3,2,1:T(8,128)(2,1)S(1)}, u32[]{:S(2)}, u32[]{:S(2)}) async-start(bf16[8,4,1,1,2048]{4,0,3,2,1:T(8,128)(2,1)} %copy.38), calls=%async_computation.3 | async-start | bytes 262144 | tf_op jit(solution)/shard_map/all_to_all | solution.py:56
  181.1 17.7 %copy-start.2 = (bf16[128,2048]{1,0:T(8,128)(2,1)S(1)}, bf16[128,2048]{1,0:T(8,128)(2,1)}, u32[]{:S(2)}) copy-start(bf16[128,2048]{1,0:T(8,128)(2,1)} %param.13) | copy-start | bytes 1572868
  181.1 17.9 %copy-start.6 = (f32[128,2]{0,1:T(2,128)S(1)}, f32[128,2]{0,1:T(2,128)}, u32[]{:S(2)}) copy-start(f32[128,2]{0,1:T(2,128)} %param.22) | copy-start | bytes 3076
  181.1 64.8 %all-to-all-start.4 = ((bf16[16,1,32,2048]{3,2,1,0:T(8,128)(2,1)}), bf16[16,1,32,2048]{3,2,1,0:T(8,128)(2,1)S(1)}, u32[]{:S(2)}, u32[]{:S(2)}) async-start(bf16[16,1,32,2048]{3,2,1,0:T(8,128)(2,1)} %stack.3), calls=%async_computation.4 | async-start | bytes 4194304 | tf_op jit(solution)/shard_map/all_to_all | solution.py:17
  204.1 6.1 %copy-start.3 = (bf16[128,512]{1,0:T(8,128)(2,1)}, bf16[128,512]{1,0:T(8,128)(2,1)S(1)}, u32[]{:S(2)}) copy-start(bf16[128,512]{1,0:T(8,128)(2,1)S(1)} %convolution_convert_fusion.2) | copy-start | bytes 393220
  204.7 30.2 %collective-permute-start = (bf16[8,512]{1,0:T(8,128)(2,1)}, bf16[8,512]{1,0:T(8,128)(2,1)S(1)}, u32[]{:S(2)}, u32[]{:S(2)}) collective-permute-start(bf16[8,512]{1,0:T(8,128)(2,1)} %get-tuple-element.6), channel_id=1, source_target_pairs={{0,1},{1,2},{2,3},{3,4},{4,5},{5,6},{6,7},{7,8},{8,9},{9,10},{10,1... | collective-permute-start | bytes 24584 | tf_op jit(solution)/shard_map/ppermute | solution.py:26
  208.3 29.4 %collective-permute-start.1 = (bf16[8,512]{1,0:T(8,128)(2,1)}, bf16[8,512]{1,0:T(8,128)(2,1)S(1)}, u32[]{:S(2)}, u32[]{:S(2)}) collective-permute-start(bf16[8,512]{1,0:T(8,128)(2,1)} %get-tuple-element.7), channel_id=1, source_target_pairs={{1,0},{2,1},{3,2},{4,3},{5,4},{6,5},{7,6},{8,7},{9,8},{10,9},{11,1... | collective-permute-start | bytes 24584 | tf_op jit(solution)/shard_map/ppermute | solution.py:29
  250.2 1.5 copy-start.4
  250.2 1.5 copy-start.5
Sparse Core Ops, SparseCore 0:
  36.5 43.6 all-gather.2
  102.9 57.5 all-gather.4
